TPU v7x, 128 devices: a whole 4x4x4 slice. The times are simulated.
128 devices in a mesh: ra: 16 (over z, x), cb: 4 (over y), dp: 2 (over core).
Axes of the slice: x: 4, y: 4, z: 4, core: 2. Of those that a mesh axis runs over, the one named last changes fastest.
Arguments:
- carried: bfloat16 [3072, 4096], P('dp', 'ra'), may hold values from -100 to 100
- branch_in: bfloat16 [3072, 4096], P('dp', 'ra'), may hold values from -12 to 12
- gain_in: float32 [4096], P('ra'), may hold values from 0.1 to 1.9
- bias_in: float32 [4096], P('ra'), may hold values from -1.8 to 1.8
- up_weight: bfloat16 [4096, 16384], P('ra', 'cb'), may hold values from -0.125 to 0.125
- down_weight: bfloat16 [16384, 4096], P('cb', 'ra'), may hold values from -0.046875 to 0.046875
- gain_out: float32 [4096], P('ra'), may hold values from 0.1 to 1.9
- bias_out: float32 [4096], P('ra'), may hold values from -1.8 to 1.8
Outputs:
- layer_out: bfloat16 [3072, 4096], P('dp', 'ra')
All inputs are finite; a program needn't handle non-finite values.
Results may differ from a plain program's by a relative error of at most 0.006.
Values may be sent and summed in bfloat16 or wider, within the bound.
A program may use at most 64 MiB of HBM per device.

v0:
```python
import jax
import jax.numpy as jnp
from jax import lax
from jax.sharding import PartitionSpec as P

residual_scale = 2.0**0.25
norm_eps = 1e-05


def copy_for_each(array, axis):
    length = lax.axis_size(axis)
    return lax.all_to_all(
        jnp.broadcast_to(array[None], (length, *array.shape)), axis, 0, 0, tiled=True
    )


def of_everyone(array, axis):
    return copy_for_each(array, axis).sum(axis=0)


def packed_total(arrays, axis):
    ravelled, at, done = (jnp.concatenate([a.reshape(-1) for a in arrays]), 0, [])
    running = of_everyone(ravelled, axis)
    for a in arrays:
        done.append(running[at : at + a.size].reshape(a.shape))
        at += a.size
    return tuple(done)


def taken_together(array, axis):
    return copy_for_each(array, axis).astype(jnp.float32).sum(axis=0)


def normalize(mixed, totals, squares, width, gain, bias):
    mean = totals[:, None] / width
    spread = squares[:, None] / width - mean * mean
    return (mixed - mean) * lax.rsqrt(spread + norm_eps) * gain + bias


def per_device(carried, branch_in, gain_in, bias_in, up_weight, down_weight, gain_out, bias_out):
    width = carried.shape[1] * lax.axis_size("ra")
    mixed_in = residual_scale * carried.astype(jnp.float32) + branch_in.astype(jnp.float32)
    totals, squares = packed_total(
        (jnp.sum(mixed_in, axis=1), jnp.sum(mixed_in * mixed_in, axis=1)), "ra"
    )
    normed = normalize(mixed_in, totals, squares, width, gain_in, bias_in).astype(jnp.bfloat16)
    regrouped = lax.all_to_all(up_weight, "ra", split_axis=1, concat_axis=0, tiled=True)
    pre_share = lax.dot_general(
        regrouped,
        lax.all_gather(normed, "ra", axis=1, tiled=True),
        (((0,), (1,)), ((), ())),
        preferred_element_type=jnp.float32,
    )
    hidden_share = jnp.square(jnp.maximum(pre_share, 0.0)).astype(jnp.bfloat16)
    branch_part = lax.dot_general(
        lax.all_gather(hidden_share, "ra", axis=0, tiled=True),
        down_weight,
        (((0,), (0,)), ((), ())),
        preferred_element_type=jnp.float32,
    )
    branch_out = taken_together(branch_part.astype(jnp.bfloat16), "cb").astype(jnp.float32)
    mixed_out = residual_scale * normed.astype(jnp.float32) + branch_out
    totals_out, squares_out = packed_total(
        (jnp.sum(mixed_out, axis=1), jnp.sum(mixed_out * mixed_out, axis=1)), "ra"
    )
    return normalize(mixed_out, totals_out, squares_out, width, gain_out, bias_out).astype(
        jnp.bfloat16
    )


def solution(mesh):
    in_specs = (
        P("dp", "ra"),
        P("dp", "ra"),
        P("ra"),
        P("ra"),
        P("ra", "cb"),
        P("cb", "ra"),
        P("ra"),
        P("ra"),
    )
    out_specs = P("dp", "ra")
    return jax.shard_map(
        per_device, mesh=mesh, in_specs=in_specs, out_specs=out_specs, check_vma=False
    )
```

profile of v0, /device:TPU:0, one launch (start us, length us, event | category | flops | bytes accessed | tf_op | source)
XLA Modules:
  0.0 324.9 jit_solution(11136814874928397678)
XLA Ops:
  6.5 0.0 copy-start
  6.5 0.0 all-gather.3.cloned.1.call-start
  6.6 2.1 fusion.3
  8.7 0.1 broadcast_in_dim.6
  8.8 16.1 %all_to_all.36 = f32[16,1,3072]{2,1,0:T(1,128)S(1)} all-to-all(f32[16,1,3072]{2,1,0:T(1,128)S(1)} %broadcast_in_dim.6), channel_id=1, replica_groups=mesh['ra'=16,'cb'=4,'dp'=2] {'ra'}, dimensions={0} | all-to-all | bytes 393216 | tf_op jit(solution)/shard_map/all_to_all | solution.py:12
  24.9 0.1 reduce_sum.65
  25.1 0.0 copy-done.3
  25.1 0.0 copy-done.4
  25.1 2.5 add_convert_fusion.1
  27.6 0.0 all-gather.3.cloned.1.call-update
  27.6 0.0 all-gather.5.cloned.1.call-start
  27.7 4.1 %copy.14 = bf16[256,4096]{0,1:T(8,128)(2,1)} copy(bf16[256,4096]{1,0:T(8,128)(2,1)} %param.12) | data formatting | bytes 4194304 | tf_op args[4]
  31.7 44.3 %all_to_all.37 = bf16[256,16,256]{0,2,1:T(8,128)(2,1)} all-to-all(bf16[256,16,256]{0,2,1:T(8,128)(2,1)} %bitcast.10), channel_id=1, replica_groups=mesh['ra'=16,'cb'=4,'dp'=2] {'ra'}, dimensions={1} | all-to-all | bytes 4194304 | tf_op jit(solution)/shard_map/all_to_all | solution.py:47
  76.0 3.9 %copy.15 = bf16[16,256,256]{2,1,0:T(8,128)(2,1)} copy(bf16[16,256,256]{1,2,0:T(8,128)(2,1)} %bitcast.9) | data formatting | bytes 4194304 | tf_op jit(solution)/shard_map/all_to_all | solution.py:47
  79.9 65.2 %all-gather.3.cloned.1.call-done = bf16[1536,4096]{1,0:T(8,128)(2,1)} async-done(((bf16[1536,256]{1,0:T(8,128)(2,1)}), bf16[1536,4096]{1,0:T(8,128)(2,1)}) %all-gather.3.cloned.1.call-update) | async-done | bytes 12582928 | tf_op jit(solution)/shard_map/all_gather | solution.py:50
  145.1 9.6 %fusion.2 = bf16[256,1536]{0,1:T(8,128)(2,1)} fusion(bf16[1536,4096]{1,0:T(8,128)(2,1)} %all-gather.3.cloned.1.call-done, bf16[4096,256]{1,0:T(8,128)(2,1)} %bitcast.11), kind=kOutput, calls=%fused_computation.5 | convolution fusion | flops 3222405120 | bytes 15466496 | tf_op jit(solution)/shard_map/dot_general | solution.py:48
  154.7 0.0 all-gather.5.cloned.1.call-update
  154.7 98.0 %all-gather.5.cloned.1.call-done = bf16[4096,1536]{0,1:T(8,128)(2,1)} async-done(((bf16[256,1536]{0,1:T(8,128)(2,1)}), bf16[4096,1536]{0,1:T(8,128)(2,1)}) %all-gather.5.cloned.1.call-update) | async-done | bytes 12582928 | tf_op jit(solution)/shard_map/all_gather | solution.py:56
  252.8 6.5 %convolution_convert_fusion = bf16[1536,256]{1,0:T(8,128)(2,1)S(1)} fusion(bf16[4096,1536]{0,1:T(8,128)(2,1)} %all-gather.5.cloned.1.call-done, bf16[4096,256]{1,0:T(8,128)(2,1)S(1)} %copy-done), kind=kOutput, calls=%fused_computation.4 | convolution fusion | flops 3221618688 | bytes 15466496 | tf_op jit(solution)/shard_map/dot_general | solution.py:55
  259.3 0.2 broadcast_in_dim.7
  259.5 40.3 %all_to_all.38 = bf16[4,1536,256]{2,1,0:T(8,128)(2,1)S(1)} all-to-all(bf16[4,1536,256]{2,1,0:T(8,128)(2,1)S(1)} %broadcast_in_dim.7), channel_id=1, replica_groups=mesh['ra'=16,'cb'=4,'dp'=2] {'cb'}, dimensions={0} | all-to-all | bytes 6291456 | tf_op jit(solution)/shard_map/all_to_all | solution.py:12
  299.8 0.5 convert_reduce_fusion
  300.2 0.0 copy-start.1
  300.2 1.1 copy-done.1
  301.4 0.0 copy-done.2
  301.4 0.5 fusion.4
  301.9 0.1 broadcast_in_dim.8
  302.0 13.1 %all_to_all.39 = f32[16,1,3072]{2,1,0:T(1,128)S(1)} all-to-all(f32[16,1,3072]{2,1,0:T(1,128)S(1)} %broadcast_in_dim.8), channel_id=1, replica_groups=mesh['ra'=16,'cb'=4,'dp'=2] {'ra'}, dimensions={0} | all-to-all | bytes 393216 | tf_op jit(solution)/shard_map/all_to_all | solution.py:12
  315.1 0.1 reduce_sum.69
  315.3 0.0 copy-done.6
  315.3 0.0 copy-done.7
  315.3 2.8 add_convert_fusion
  (12 shorter events, 0.0 us)
Async XLA Ops:
  6.5 246.2 %copy-start = (bf16[4096,256]{1,0:T(8,128)(2,1)S(1)}, bf16[4096,256]{1,0:T(8,128)(2,1)}, u32[]{:S(2)}) copy-start(bf16[4096,256]{1,0:T(8,128)(2,1)} %param.13) | copy-start | bytes 6291460
  6.5 18.5 %copy-start.3 = (bf16[1536,256]{1,0:T(8,128)(2,1)S(1)}, bf16[1536,256]{1,0:T(8,128)(2,1)}, u32[]{:S(2)}) copy-start(bf16[1536,256]{1,0:T(8,128)(2,1)} %param.9) | copy-start | bytes 2359300
  6.5 18.5 %copy-start.4 = (f32[256]{0:T(256)S(1)}, f32[256]{0:T(256)}, u32[]{:S(2)}) copy-start(f32[256]{0:T(256)} %param.11) | copy-start | bytes 3076
  6.5 18.5 %copy-start.5 = (f32[256]{0:T(256)S(1)}, f32[256]{0:T(256)}, u32[]{:S(2)}) copy-start(f32[256]{0:T(256)} %param.10) | copy-start | bytes 3076
  6.5 138.6 %all-gather.3.cloned.1.call-start = ((), (), s32[]{:S(2)}) async-start(), calls=%async_computation.4 | async-start | bytes 13369344 | tf_op jit(solution)/shard_map/all_gather | solution.py:50
  27.6 225.1 %all-gather.5.cloned.1.call-start = ((), (), s32[]{:S(2)}) async-start(), calls=%async_computation.5 | async-start | bytes 13369344 | tf_op jit(solution)/shard_map/all_gather | solution.py:56
  299.8 1.6 copy-start.2
  300.2 1.2 copy-start.1
  301.4 13.9 %copy-start.6 = (f32[256]{0:T(256)S(1)}, f32[256]{0:T(256)}, u32[]{:S(2)}) copy-start(f32[256]{0:T(256)} %param.15) | copy-start | bytes 3076
  301.4 13.9 %copy-start.7 = (f32[256]{0:T(256)S(1)}, f32[256]{0:T(256)}, u32[]{:S(2)}) copy-start(f32[256]{0:T(256)} %param.14) | copy-start | bytes 3076
Sparse Core Ops, SparseCore 0:
  27.7 117.3 all-gather.2
  154.9 97.8 all-gather.4
where the time goes:
time: 325 us
  waiting for transfers between devices  163 us (50%)
  blocking collectives  114 us (35%)
  matrix products  16.1 us (5%)
  between operations  13.5 us (4%)
  local copies, waits for them, and re-layouts  9.57 us (3%)
  other arithmetic  8.59 us (3%)
    all_gather x1, waiting for transfers between devices, per_device(): lax.all_gather(hidden_share, 'ra', axis=0, tiled=True)  98 us
    all_to_all x3, blocking collectives, copy_for_each(): lax.all_to_all(jnp.broadcast_to(array[None], (length, *array.shape)), axi...  69.5 us
    all_gather x1, waiting for transfers between devices, per_device(): lax.all_gather(normed, 'ra', axis=1, tiled=True)  65.2 us
    all_to_all x1, blocking collectives, per_device(): lax.all_to_all(up_weight, 'ra', split_axis=1, concat_axis=0, tiled=True)  44.3 us
    dot_general x1, matrix products, per_device(): lax.dot_general(regrouped, lax.all_gather(normed, 'ra', axis=1, tiled=Tru...  9.57 us
  transfers between devices with their start and end apart: 2, of which 2 were waited for; matrix products, arithmetic and copies ran while one was open for 2% of the time, Pallas kernels for 0%

commit v1 on v0

--- a/solution.py
+++ b/solution.py
@@ -1,3 +1,4 @@
+import functools
 import jax
 import jax.numpy as jnp
 from jax import lax
@@ -5,6 +6,24 @@
 
 residual_scale = 2.0**0.25
 norm_eps = 1e-05
+
+
+def ratios_hold(own_rows, comm_axis):
+    piece_next = lax.psum(1, comm_axis)
+    latest = lax.axis_index(comm_axis)
+    w1, arr_next, everything = (piece_next, latest, own_rows.shape[1])
+    chunks = tuple(((u, (u + 1) % w1) for u in range(w1)))
+    earlier = own_rows
+    ready = jnp.zeros((*own_rows.shape[:1], w1 * everything, *own_rows.shape[2:]), own_rows.dtype)
+    for jj in range(w1):
+        mixed_arr = (arr_next - jj) % w1
+        ready = lax.dynamic_update_slice_in_dim(ready, earlier, mixed_arr * everything, axis=1)
+        if jj < w1 - 1:
+            earlier = lax.ppermute(earlier, comm_axis, chunks)
+    return ready
+
+
+set_things = functools.partial(ratios_hold, comm_axis="ra")
 
 
 def copy_for_each(array, axis):
@@ -46,10 +65,7 @@
     normed = normalize(mixed_in, totals, squares, width, gain_in, bias_in).astype(jnp.bfloat16)
     regrouped = lax.all_to_all(up_weight, "ra", split_axis=1, concat_axis=0, tiled=True)
     pre_share = lax.dot_general(
-        regrouped,
-        lax.all_gather(normed, "ra", axis=1, tiled=True),
-        (((0,), (1,)), ((), ())),
-        preferred_element_type=jnp.float32,
+        regrouped, set_things(normed), (((0,), (1,)), ((), ())), preferred_element_type=jnp.float32
     )
     hidden_share = jnp.square(jnp.maximum(pre_share, 0.0)).astype(jnp.bfloat16)
     branch_part = lax.dot_general(

time: 325 us -> 516 us (1.59)
  waiting for transfers between devices: 163 us -> 364 us
  blocking collectives: 114 us -> 53.4 us
  local copies, waits for them, and re-layouts: 9.57 us -> 47.8 us
  starting transfers between devices: 0.08 us -> 15.4 us
    ppermute x0 -> x15, waiting for transfers between devices: none -> 260 us  [ratios_hold(): earlier = lax.ppermute(earlier, comm_axis, chunks)]
    all_gather x1 -> x0, waiting for transfers between devices: 65.2 us -> none  [per_device(): lax.all_gather(normed, 'ra', axis=1, tiled=True)]
    all_to_all x1 -> x0, blocking collectives: 44.3 us -> none  [per_device(): lax.all_to_all(up_weight, 'ra', split_axis=1, concat_axis=0, tiled=True)]
    dynamic_update_slice x0 -> x15, local copies, waits for them, and re-layouts: none -> 24.2 us  [ratios_hold(): lax.dynamic_update_slice_in_dim(ready, earlier, mixed_arr * everything, a...]
    all_to_all x3 -> x2, blocking collectives: 69.5 us -> 53.4 us  [copy_for_each(): lax.all_to_all(jnp.broadcast_to(array[None], (length, *array.shape)), axi...]
    all_to_all x0 -> x2, starting transfers between devices: none -> 14.8 us  [the longest x1 7.99 us: copy_for_each(): lax.all_to_all(jnp.broadcast_to(array[None], (length, *array.shape)), axi...]
    all_to_all x0 -> x2, waiting for transfers between devices: none -> 8.33 us  [the longest x1 8.32 us: copy_for_each(): lax.all_to_all(jnp.broadcast_to(array[None], (length, *array.shape)), axi...]
    unnamed x17 -> x43, local copies, waits for them, and re-layouts: 5.25 us -> 12.4 us
  transfers between devices with their start and end apart: 2 -> 18, of which waited for: 2 -> 17; matrix products, arithmetic and copies ran while one was open for 2% -> 6% of each run, Pallas kernels for 0% -> 0%
where the time goes in v1:
time: 516 us; the launch traced here: 515 us
  waiting for transfers between devices  364 us (71%)
  blocking collectives  53.4 us (10%)
  local copies, waits for them, and re-layouts  47.8 us (9%)
  starting transfers between devices  15.4 us (3%)
  matrix products  13.9 us (3%)
  between operations  13.6 us (3%)
  other arithmetic  7.56 us (1%)
    ppermute x15, waiting for transfers between devices, ratios_hold(): earlier = lax.ppermute(earlier, comm_axis, chunks)  260 us
    all_gather x1, waiting for transfers between devices, per_device(): lax.all_gather(hidden_share, 'ra', axis=0, tiled=True)  95.2 us
    all_to_all x2, blocking collectives, copy_for_each(): lax.all_to_all(jnp.broadcast_to(array[None], (length, *array.shape)), axi...  53.4 us
    dynamic_update_slice x15, local copies, waits for them, and re-layouts, ratios_hold(): lax.dynamic_update_slice_in_dim(ready, earlier, mixed_arr * everything, a...  24.2 us
    unnamed x43, local copies, waits for them, and re-layouts  12.4 us
  transfers between devices with their start and end apart: 18, of which 17 were waited for; matrix products, arithmetic and copies ran while one was open for 6% of the time, Pallas kernels for 0%

profile of v1, /device:TPU:0, one launch (start us, length us, event | category | flops | bytes accessed | tf_op | source)
XLA Modules:
  0.0 515.3 jit_solution(12768475944955270042)
XLA Ops:
  9.4 8.0 %all-to-all-start = ((f32[16,1,3072]{2,1,0:T(1,128)}), f32[16,1,3072]{2,1,0:T(1,128)S(1)}, u32[]{:S(2)}, u32[]{:S(2)}) async-start(f32[16,1,3072]{2,1,0:T(1,128)} %broadcast_in_dim.8), calls=%async_computation | async-start | bytes 393216 | tf_op jit(solution)/shard_map/all_to_all | solution.py:31
  17.4 8.3 %all-to-all-done = f32[16,1,3072]{2,1,0:T(1,128)S(1)} async-done(((f32[16,1,3072]{2,1,0:T(1,128)}), f32[16,1,3072]{2,1,0:T(1,128)S(1)}, u32[]{:S(2)}, u32[]{:S(2)}) %all-to-all-start) | async-done | bytes 196640 | tf_op jit(solution)/shard_map/all_to_all | solution.py:31
  25.9 6.1 %broadcast_in_dim.9 = bf16[1536,4096]{1,0:T(8,128)(2,1)} broadcast(bf16[]{:T(256)} %constant.121.clone.1), dimensions={} | broadcast | bytes 12582914 | tf_op jit(solution)/shard_map/broadcast_in_dim | solution.py:17
  34.1 20.6 %collective-permute-done = bf16[1536,256]{1,0:T(8,128)(2,1)S(1)} collective-permute-done((bf16[1536,256]{1,0:T(8,128)(2,1)S(1)}, bf16[1536,256]{1,0:T(8,128)(2,1)S(1)}, u32[]{:S(2)}, u32[]{:S(2)}) %collective-permute-start) | collective-permute-done | bytes 786464 | tf_op jit(solution)/shard_map/ppermute | solution.py:22
  55.6 19.4 %collective-permute-done.1 = bf16[1536,256]{1,0:T(8,128)(2,1)S(1)} collective-permute-done((bf16[1536,256]{1,0:T(8,128)(2,1)S(1)}, bf16[1536,256]{1,0:T(8,128)(2,1)S(1)}, u32[]{:S(2)}, u32[]{:S(2)}) %collective-permute-start.1) | collective-permute-done | bytes 786464 | tf_op jit(solution)/shard_map/ppermute | solution.py:22
  75.9 18.5 %collective-permute-done.2 = bf16[1536,256]{1,0:T(8,128)(2,1)S(1)} collective-permute-done((bf16[1536,256]{1,0:T(8,128)(2,1)S(1)}, bf16[1536,256]{1,0:T(8,128)(2,1)S(1)}, u32[]{:S(2)}, u32[]{:S(2)}) %collective-permute-start.2) | collective-permute-done | bytes 786464 | tf_op jit(solution)/shard_map/ppermute | solution.py:22
  95.3 18.6 %collective-permute-done.3 = bf16[1536,256]{1,0:T(8,128)(2,1)S(1)} collective-permute-done((bf16[1536,256]{1,0:T(8,128)(2,1)S(1)}, bf16[1536,256]{1,0:T(8,128)(2,1)S(1)}, u32[]{:S(2)}, u32[]{:S(2)}) %collective-permute-start.3) | collective-permute-done | bytes 786464 | tf_op jit(solution)/shard_map/ppermute | solution.py:22
  114.8 17.7 %collective-permute-done.4 = bf16[1536,256]{1,0:T(8,128)(2,1)S(1)} collective-permute-done((bf16[1536,256]{1,0:T(8,128)(2,1)S(1)}, bf16[1536,256]{1,0:T(8,128)(2,1)S(1)}, u32[]{:S(2)}, u32[]{:S(2)}) %collective-permute-start.4) | collective-permute-done | bytes 786464 | tf_op jit(solution)/shard_map/ppermute | solution.py:22
  133.5 16.8 %collective-permute-done.5 = bf16[1536,256]{1,0:T(8,128)(2,1)S(1)} collective-permute-done((bf16[1536,256]{1,0:T(8,128)(2,1)S(1)}, bf16[1536,256]{1,0:T(8,128)(2,1)S(1)}, u32[]{:S(2)}, u32[]{:S(2)}) %collective-permute-start.5) | collective-permute-done | bytes 786464 | tf_op jit(solution)/shard_map/ppermute | solution.py:22
  151.2 15.9 %collective-permute-done.6 = bf16[1536,256]{1,0:T(8,128)(2,1)S(1)} collective-permute-done((bf16[1536,256]{1,0:T(8,128)(2,1)S(1)}, bf16[1536,256]{1,0:T(8,128)(2,1)S(1)}, u32[]{:S(2)}, u32[]{:S(2)}) %collective-permute-start.6) | collective-permute-done | bytes 786464 | tf_op jit(solution)/shard_map/ppermute | solution.py:22
  168.0 17.2 %collective-permute-done.7 = bf16[1536,256]{1,0:T(8,128)(2,1)S(1)} collective-permute-done((bf16[1536,256]{1,0:T(8,128)(2,1)S(1)}, bf16[1536,256]{1,0:T(8,128)(2,1)S(1)}, u32[]{:S(2)}, u32[]{:S(2)}) %collective-permute-start.7) | collective-permute-done | bytes 786464 | tf_op jit(solution)/shard_map/ppermute | solution.py:22
  186.1 19.1 %collective-permute-done.8 = bf16[1536,256]{1,0:T(8,128)(2,1)} collective-permute-done((bf16[1536,256]{1,0:T(8,128)(2,1)S(1)}, bf16[1536,256]{1,0:T(8,128)(2,1)}, u32[]{:S(2)}, u32[]{:S(2)}) %collective-permute-start.8) | collective-permute-done | bytes 786464 | tf_op jit(solution)/shard_map/ppermute | solution.py:22
  205.2 4.1 copy.14
  209.3 6.8 %all-to-all-start.1 = ((bf16[256,16,256]{0,2,1:T(8,128)(2,1)}), bf16[256,16,256]{0,2,1:T(8,128)(2,1)}, u32[]{:S(2)}, u32[]{:S(2)}) async-start(bf16[256,16,256]{0,2,1:T(8,128)(2,1)} %bitcast.9), calls=%async_computation.1 | async-start | bytes 4194304 | tf_op jit(solution)/shard_map/all_to_all | solution.py:66
  216.1 22.2 %collective-permute-done.9 = bf16[1536,256]{1,0:T(8,128)(2,1)} collective-permute-done((bf16[1536,256]{1,0:T(8,128)(2,1)}, bf16[1536,256]{1,0:T(8,128)(2,1)}, u32[]{:S(2)}, u32[]{:S(2)}) %collective-permute-start.9) | collective-permute-done | bytes 786464 | tf_op jit(solution)/shard_map/ppermute | solution.py:22
  238.3 23.7 %collective-permute-done.10 = bf16[1536,256]{1,0:T(8,128)(2,1)} collective-permute-done((bf16[1536,256]{1,0:T(8,128)(2,1)}, bf16[1536,256]{1,0:T(8,128)(2,1)}, u32[]{:S(2)}, u32[]{:S(2)}) %collective-permute-start.10) | collective-permute-done | bytes 786464 | tf_op jit(solution)/shard_map/ppermute | solution.py:22
  261.9 2.1 constant_dynamic-update-slice_fusion.14
  264.1 2.1 constant_dynamic-update-slice_fusion.13
  266.2 3.9 copy.15
  270.1 11.3 %collective-permute-done.11 = bf16[1536,256]{1,0:T(8,128)(2,1)} collective-permute-done((bf16[1536,256]{1,0:T(8,128)(2,1)}, bf16[1536,256]{1,0:T(8,128)(2,1)}, u32[]{:S(2)}, u32[]{:S(2)}) %collective-permute-start.11) | collective-permute-done | bytes 786464 | tf_op jit(solution)/shard_map/ppermute | solution.py:22
  281.5 2.1 constant_dynamic-update-slice_fusion.12
  283.6 2.2 constant_dynamic-update-slice_fusion.11
  287.8 14.6 %collective-permute-done.12 = bf16[1536,256]{1,0:T(8,128)(2,1)S(1)} collective-permute-done((bf16[1536,256]{1,0:T(8,128)(2,1)}, bf16[1536,256]{1,0:T(8,128)(2,1)S(1)}, u32[]{:S(2)}, u32[]{:S(2)}) %collective-permute-start.12) | collective-permute-done | bytes 786464 | tf_op jit(solution)/shard_map/ppermute | solution.py:22
  308.6 15.6 %collective-permute-done.13 = bf16[1536,256]{1,0:T(8,128)(2,1)S(1)} collective-permute-done((bf16[1536,256]{1,0:T(8,128)(2,1)S(1)}, bf16[1536,256]{1,0:T(8,128)(2,1)S(1)}, u32[]{:S(2)}, u32[]{:S(2)}) %collective-permute-start.13) | collective-permute-done | bytes 786464 | tf_op jit(solution)/shard_map/ppermute | solution.py:22
  326.3 2.3 constant_dynamic-update-slice_fusion.3
  330.6 8.9 %collective-permute-done.14 = bf16[1536,256]{1,0:T(8,128)(2,1)S(1)} collective-permute-done((bf16[1536,256]{1,0:T(8,128)(2,1)S(1)}, bf16[1536,256]{1,0:T(8,128)(2,1)S(1)}, u32[]{:S(2)}, u32[]{:S(2)}) %collective-permute-start.14) | collective-permute-done | bytes 786464 | tf_op jit(solution)/shard_map/ppermute | solution.py:22
  340.5 7.4 %fusion.2 = bf16[256,1536]{0,1:T(8,128)(2,1)} fusion(bf16[1536,4096]{1,0:T(8,128)(2,1)} %constant_dynamic-update-slice_fusion, bf16[4096,256]{1,0:T(8,128)(2,1)S(1)} %bitcast.10), kind=kOutput, calls=%fused_computation.5 | convolution fusion | flops 3222405120 | bytes 15466496 | tf_op jit(solution)/shard_map/dot_general | solution.py:67
  348.0 95.2 %all-gather.2.cloned.1.call-done = bf16[4096,1536]{0,1:T(8,128)(2,1)} async-done(((bf16[256,1536]{0,1:T(8,128)(2,1)}), bf16[4096,1536]{0,1:T(8,128)(2,1)}) %all-gather.2.cloned.1.call-update) | async-done | bytes 12582928 | tf_op jit(solution)/shard_map/all_gather | solution.py:72
  443.2 6.5 %convolution_convert_fusion = bf16[1536,256]{1,0:T(8,128)(2,1)S(1)} fusion(bf16[4096,1536]{0,1:T(8,128)(2,1)} %all-gather.2.cloned.1.call-done, bf16[4096,256]{1,0:T(8,128)(2,1)S(1)} %copy-done), kind=kOutput, calls=%fused_computation.4 | convolution fusion | flops 3221618688 | bytes 15466496 | tf_op jit(solution)/shard_map/dot_general | solution.py:71
  449.9 40.3 %all_to_all.36 = bf16[4,1536,256]{2,1,0:T(8,128)(2,1)S(1)} all-to-all(bf16[4,1536,256]{2,1,0:T(8,128)(2,1)S(1)} %broadcast_in_dim.10), channel_id=1, replica_groups=mesh['ra'=16,'cb'=4,'dp'=2] {'cb'}, dimensions={0} | all-to-all | bytes 6291456 | tf_op jit(solution)/shard_map/all_to_all | solution.py:31
  492.5 13.1 %all_to_all.37 = f32[16,1,3072]{2,1,0:T(1,128)S(1)} all-to-all(f32[16,1,3072]{2,1,0:T(1,128)S(1)} %broadcast_in_dim.11), channel_id=1, replica_groups=mesh['ra'=16,'cb'=4,'dp'=2] {'ra'}, dimensions={0} | all-to-all | bytes 393216 | tf_op jit(solution)/shard_map/all_to_all | solution.py:31
  505.7 2.8 add_convert_fusion
  (83 shorter events, 28.2 us)
Async XLA Ops:
  6.5 436.6 %copy-start = (bf16[4096,256]{1,0:T(8,128)(2,1)S(1)}, bf16[4096,256]{1,0:T(8,128)(2,1)}, u32[]{:S(2)}) copy-start(bf16[4096,256]{1,0:T(8,128)(2,1)} %param.13) | copy-start | bytes 6291460
  9.4 16.3 %all-to-all-start = ((f32[16,1,3072]{2,1,0:T(1,128)}), f32[16,1,3072]{2,1,0:T(1,128)S(1)}, u32[]{:S(2)}, u32[]{:S(2)}) async-start(f32[16,1,3072]{2,1,0:T(1,128)} %broadcast_in_dim.8), calls=%async_computation | async-start | bytes 393216 | tf_op jit(solution)/shard_map/all_to_all | solution.py:31
  25.9 6.2 %copy-start.2 = (bf16[1536,256]{1,0:T(8,128)(2,1)S(1)}, bf16[1536,256]{1,0:T(8,128)(2,1)}, u32[]{:S(2)}) copy-start(bf16[1536,256]{1,0:T(8,128)(2,1)} %param.9) | copy-start | bytes 2359300
  25.9 6.2 %copy-start.3 = (bf16[1536,256]{1,0:T(8,128)(2,1)S(1)}, bf16[1536,256]{1,0:T(8,128)(2,1)}, u32[]{:S(2)}) copy-start(bf16[1536,256]{1,0:T(8,128)(2,1)} %param.8) | copy-start | bytes 2359300
  25.9 6.1 %copy-start.17 = (f32[256]{0:T(256)S(1)}, f32[256]{0:T(256)}, u32[]{:S(2)}) copy-start(f32[256]{0:T(256)} %param.11) | copy-start | bytes 3076
  25.9 6.1 %copy-start.18 = (f32[256]{0:T(256)S(1)}, f32[256]{0:T(256)}, u32[]{:S(2)}) copy-start(f32[256]{0:T(256)} %param.10) | copy-start | bytes 3076
  33.5 21.2 %collective-permute-start = (bf16[1536,256]{1,0:T(8,128)(2,1)S(1)}, bf16[1536,256]{1,0:T(8,128)(2,1)S(1)}, u32[]{:S(2)}, u32[]{:S(2)}) collective-permute-start(bf16[1536,256]{1,0:T(8,128)(2,1)S(1)} %get-tuple-element.10), channel_id=1, source_target_pairs={{0,8},{8,16},{16,24},{24,32},{32,40},{40,48},{48,56},{56,64},{64,7... | collective-permute-start | bytes 2359304 | tf_op jit(solution)/shard_map/ppermute | solution.py:22
  54.7 20.3 %collective-permute-start.1 = (bf16[1536,256]{1,0:T(8,128)(2,1)S(1)}, bf16[1536,256]{1,0:T(8,128)(2,1)S(1)}, u32[]{:S(2)}, u32[]{:S(2)}) collective-permute-start(bf16[1536,256]{1,0:T(8,128)(2,1)S(1)} %collective-permute-done), channel_id=1, source_target_pairs={{0,8},{8,16},{16,24},{24,32},{32,40},{40,48},{48,56},{56,64},{64,7... | collective-permute-start | bytes 2359304 | tf_op jit(solution)/shard_map/ppermute | solution.py:22
  75.0 0.9 copy-start.16
  75.0 19.5 %collective-permute-start.2 = (bf16[1536,256]{1,0:T(8,128)(2,1)S(1)}, bf16[1536,256]{1,0:T(8,128)(2,1)S(1)}, u32[]{:S(2)}, u32[]{:S(2)}) collective-permute-start(bf16[1536,256]{1,0:T(8,128)(2,1)S(1)} %collective-permute-done.1), channel_id=1, source_target_pairs={{0,8},{8,16},{16,24},{24,32},{32,40},{40,48},{48,56},{56,64},{64,7... | collective-permute-start | bytes 2359304 | tf_op jit(solution)/shard_map/ppermute | solution.py:22
  95.3 18.6 %collective-permute-start.3 = (bf16[1536,256]{1,0:T(8,128)(2,1)S(1)}, bf16[1536,256]{1,0:T(8,128)(2,1)S(1)}, u32[]{:S(2)}, u32[]{:S(2)}) collective-permute-start(bf16[1536,256]{1,0:T(8,128)(2,1)S(1)} %collective-permute-done.2), channel_id=1, source_target_pairs={{0,8},{8,16},{16,24},{24,32},{32,40},{40,48},{48,56},{56,64},{64,7... | collective-permute-start | bytes 2359304 | tf_op jit(solution)/shard_map/ppermute | solution.py:22
  114.8 17.7 %collective-permute-start.4 = (bf16[1536,256]{1,0:T(8,128)(2,1)S(1)}, bf16[1536,256]{1,0:T(8,128)(2,1)S(1)}, u32[]{:S(2)}, u32[]{:S(2)}) collective-permute-start(bf16[1536,256]{1,0:T(8,128)(2,1)S(1)} %collective-permute-done.3), channel_id=1, source_target_pairs={{0,8},{8,16},{16,24},{24,32},{32,40},{40,48},{48,56},{56,64},{64,7... | collective-permute-start | bytes 2359304 | tf_op jit(solution)/shard_map/ppermute | solution.py:22
  132.6 17.7 %collective-permute-start.5 = (bf16[1536,256]{1,0:T(8,128)(2,1)S(1)}, bf16[1536,256]{1,0:T(8,128)(2,1)S(1)}, u32[]{:S(2)}, u32[]{:S(2)}) collective-permute-start(bf16[1536,256]{1,0:T(8,128)(2,1)S(1)} %collective-permute-done.4), channel_id=1, source_target_pairs={{0,8},{8,16},{16,24},{24,32},{32,40},{40,48},{48,56},{56,64},{64,7... | collective-permute-start | bytes 2359304 | tf_op jit(solution)/shard_map/ppermute | solution.py:22
  150.3 16.8 %collective-permute-start.6 = (bf16[1536,256]{1,0:T(8,128)(2,1)S(1)}, bf16[1536,256]{1,0:T(8,128)(2,1)S(1)}, u32[]{:S(2)}, u32[]{:S(2)}) collective-permute-start(bf16[1536,256]{1,0:T(8,128)(2,1)S(1)} %collective-permute-done.5), channel_id=1, source_target_pairs={{0,8},{8,16},{16,24},{24,32},{32,40},{40,48},{48,56},{56,64},{64,7... | collective-permute-start | bytes 2359304 | tf_op jit(solution)/shard_map/ppermute | solution.py:22
  168.0 17.2 %collective-permute-start.7 = (bf16[1536,256]{1,0:T(8,128)(2,1)S(1)}, bf16[1536,256]{1,0:T(8,128)(2,1)S(1)}, u32[]{:S(2)}, u32[]{:S(2)}) collective-permute-start(bf16[1536,256]{1,0:T(8,128)(2,1)S(1)} %collective-permute-done.6), channel_id=1, source_target_pairs={{0,8},{8,16},{16,24},{24,32},{32,40},{40,48},{48,56},{56,64},{64,7... | collective-permute-start | bytes 2359304 | tf_op jit(solution)/shard_map/ppermute | solution.py:22
  186.1 19.1 %collective-permute-start.8 = (bf16[1536,256]{1,0:T(8,128)(2,1)S(1)}, bf16[1536,256]{1,0:T(8,128)(2,1)}, u32[]{:S(2)}, u32[]{:S(2)}) collective-permute-start(bf16[1536,256]{1,0:T(8,128)(2,1)S(1)} %collective-permute-done.7), channel_id=1, source_target_pairs={{0,8},{8,16},{16,24},{24,32},{32,40},{40,48},{48,56},{56,64},{64,7... | collective-permute-start | bytes 2359304 | tf_op jit(solution)/shard_map/ppermute | solution.py:22
  205.2 33.1 %collective-permute-start.9 = (bf16[1536,256]{1,0:T(8,128)(2,1)}, bf16[1536,256]{1,0:T(8,128)(2,1)}, u32[]{:S(2)}, u32[]{:S(2)}) collective-permute-start(bf16[1536,256]{1,0:T(8,128)(2,1)} %collective-permute-done.8), channel_id=1, source_target_pairs={{0,8},{8,16},{16,24},{24,32},{32,40},{40,48},{48,56},{56,64},{64,7... | collective-permute-start | bytes 2359304 | tf_op jit(solution)/shard_map/ppermute | solution.py:22
  209.3 56.9 %all-to-all-start.1 = ((bf16[256,16,256]{0,2,1:T(8,128)(2,1)}), bf16[256,16,256]{0,2,1:T(8,128)(2,1)}, u32[]{:S(2)}, u32[]{:S(2)}) async-start(bf16[256,16,256]{0,2,1:T(8,128)(2,1)} %bitcast.9), calls=%async_computation.1 | async-start | bytes 4194304 | tf_op jit(solution)/shard_map/all_to_all | solution.py:66
  216.0 227.1 %all-gather.2.cloned.1.call-start = ((), (), s32[]{:S(2)}) async-start(), calls=%async_computation.4 | async-start | bytes 13369344 | tf_op jit(solution)/shard_map/all_gather | solution.py:72
  238.3 23.7 %collective-permute-start.10 = (bf16[1536,256]{1,0:T(8,128)(2,1)}, bf16[1536,256]{1,0:T(8,128)(2,1)}, u32[]{:S(2)}, u32[]{:S(2)}) collective-permute-start(bf16[1536,256]{1,0:T(8,128)(2,1)} %collective-permute-done.9), channel_id=1, source_target_pairs={{0,8},{8,16},{16,24},{24,32},{32,40},{40,48},{48,56},{56,64},{64,7... | collective-permute-start | bytes 2359304 | tf_op jit(solution)/shard_map/ppermute | solution.py:22
  261.9 19.5 %collective-permute-start.11 = (bf16[1536,256]{1,0:T(8,128)(2,1)}, bf16[1536,256]{1,0:T(8,128)(2,1)}, u32[]{:S(2)}, u32[]{:S(2)}) collective-permute-start(bf16[1536,256]{1,0:T(8,128)(2,1)} %collective-permute-done.10), channel_id=1, source_target_pairs={{0,8},{8,16},{16,24},{24,32},{32,40},{40,48},{48,56},{56,64},{64,7... | collective-permute-start | bytes 2359304 | tf_op jit(solution)/shard_map/ppermute | solution.py:22
  270.1 15.7 %copy-start.10 = (bf16[1536,256]{1,0:T(8,128)(2,1)S(1)}, bf16[1536,256]{1,0:T(8,128)(2,1)}, u32[]{:S(2)}) copy-start(bf16[1536,256]{1,0:T(8,128)(2,1)} %copy-done.9) | copy-start | bytes 2359300
  270.1 16.6 %copy-start.15 = (bf16[1536,256]{1,0:T(8,128)(2,1)S(1)}, bf16[1536,256]{1,0:T(8,128)(2,1)}, u32[]{:S(2)}) copy-start(bf16[1536,256]{1,0:T(8,128)(2,1)} %copy-done.14) | copy-start | bytes 2359300
  270.1 32.2 %copy-start.8 = (bf16[1536,256]{1,0:T(8,128)(2,1)S(1)}, bf16[1536,256]{1,0:T(8,128)(2,1)}, u32[]{:S(2)}) copy-start(bf16[1536,256]{1,0:T(8,128)(2,1)} %copy-done.7) | copy-start | bytes 2359300
  281.5 20.9 %collective-permute-start.12 = (bf16[1536,256]{1,0:T(8,128)(2,1)}, bf16[1536,256]{1,0:T(8,128)(2,1)S(1)}, u32[]{:S(2)}, u32[]{:S(2)}) collective-permute-start(bf16[1536,256]{1,0:T(8,128)(2,1)} %collective-permute-done.11), channel_id=1, source_target_pairs={{0,8},{8,16},{16,24},{24,32},{32,40},{40,48},{48,56},{56,64},{64,7... | collective-permute-start | bytes 2359304 | tf_op jit(solution)/shard_map/ppermute | solution.py:22
  283.6 19.8 %copy-start.13 = (bf16[1536,256]{1,0:T(8,128)(2,1)S(1)}, bf16[1536,256]{1,0:T(8,128)(2,1)}, u32[]{:S(2)}) copy-start(bf16[1536,256]{1,0:T(8,128)(2,1)} %copy-done.12) | copy-start | bytes 2359300
  302.4 21.8 %collective-permute-start.13 = (bf16[1536,256]{1,0:T(8,128)(2,1)S(1)}, bf16[1536,256]{1,0:T(8,128)(2,1)S(1)}, u32[]{:S(2)}, u32[]{:S(2)}) collective-permute-start(bf16[1536,256]{1,0:T(8,128)(2,1)S(1)} %collective-permute-done.12), channel_id=1, source_target_pairs={{0,8},{8,16},{16,24},{24,32},{32,40},{40,48},{48,56},{56,64},{64,7... | collective-permute-start | bytes 2359304 | tf_op jit(solution)/shard_map/ppermute | solution.py:22
  324.2 15.3 %collective-permute-start.14 = (bf16[1536,256]{1,0:T(8,128)(2,1)S(1)}, bf16[1536,256]{1,0:T(8,128)(2,1)S(1)}, u32[]{:S(2)}, u32[]{:S(2)}) collective-permute-start(bf16[1536,256]{1,0:T(8,128)(2,1)S(1)} %collective-permute-done.13), channel_id=1, source_target_pairs={{0,8},{8,16},{16,24},{24,32},{32,40},{40,48},{48,56},{56,64},{64,7... | collective-permute-start | bytes 2359304 | tf_op jit(solution)/shard_map/ppermute | solution.py:22
  326.3 14.2 %copy-start.4 = (bf16[16,256,256]{2,1,0:T(8,128)(2,1)S(1)}, bf16[16,256,256]{2,1,0:T(8,128)(2,1)}, u32[]{:S(2)}) copy-start(bf16[16,256,256]{2,1,0:T(8,128)(2,1)} %copy.15) | copy-start | bytes 6291460
  490.2 15.5 %copy-start.19 = (f32[256]{0:T(256)S(1)}, f32[256]{0:T(256)}, u32[]{:S(2)}) copy-start(f32[256]{0:T(256)} %param.15) | copy-start | bytes 3076
  490.2 15.5 %copy-start.20 = (f32[256]{0:T(256)S(1)}, f32[256]{0:T(256)}, u32[]{:S(2)}) copy-start(f32[256]{0:T(256)} %param.14) | copy-start | bytes 3076
  490.6 1.2 copy-start.1
  (7 other events, 6.2 us)
Sparse Core Ops, SparseCore 0:
  348.1 95.0 all-gather.1
